TPU v7x, 32 devices: a whole 2x2x4 slice. The times are simulated.
32 devices in a mesh: sp: 8 (over z, y), tp: 4 (over x, core).
Axes of the slice: x: 2, y: 2, z: 4, core: 2. Of those that a mesh axis runs over, the one named last changes fastest.
Arguments:
- resid: bfloat16 [6144, 2048], P(('sp', 'tp')), may hold values from -6 to 6
- query_small: bfloat16 [6144, 768], P('sp', 'tp'), may hold values from -480 to 480
- query_large: bfloat16 [6144, 1280], P('sp', 'tp'), may hold values from -480 to 480
- kv_latent: bfloat16 [6144, 256], P('sp'), may hold values from -6 to 6
- rope_key: bfloat16 [6144, 32], P('sp'), may hold values from -6 to 6
- kv_gain: bfloat16 [256], replicated, may hold values from 0.099609375 to 1.8984375
- up_key_small: bfloat16 [256, 512], P(None, 'tp'), may hold values from -0.375 to 0.375
- up_value_small: bfloat16 [256, 512], P(None, 'tp'), may hold values from -0.375 to 0.375
- up_key_large: bfloat16 [256, 1024], P(None, 'tp'), may hold values from -0.375 to 0.375
- up_value_large: bfloat16 [256, 1024], P(None, 'tp'), may hold values from -0.375 to 0.375
- out_weight: bfloat16 [1536, 2048], replicated, may hold values from -0.359375 to 0.359375
- mix_gain: bfloat16 [2048], replicated, may hold values from 0.099609375 to 1.8984375
- gate_weight: bfloat16 [2048, 5632], P('sp', 'tp'), may hold values from -0.125 to 0.125
- up_weight: bfloat16 [2048, 5632], P('sp', 'tp'), may hold values from -0.125 to 0.125
- down_weight: bfloat16 [2048, 5632], P('sp', 'tp'), may hold values from -0.078125 to 0.078125
Outputs:
- layer_output: bfloat16 [6144, 2048], P(('sp', 'tp'))
All inputs are finite; a program needn't handle non-finite values.
Results may differ from a plain program's by a relative error of at most 0.014.
The roundings to bfloat16 on the way count: a program that leaves them out, or rounds other values in their place, can miss the bound.
Values may be sent and summed in bfloat16 or wider, within the bound.
A program may use at most 128 MiB of HBM per device.

v0:
```python
import math

import jax
import jax.numpy as jnp
from jax import lax
from jax.sharding import PartitionSpec as P

HEADS_SMALL = 8
NOPE_SMALL = 64
NOPE_LARGE = 128
VALUE_SMALL = 64
VALUE_LARGE = 128
ROTARY = 32


THETA = 10000.0
EPSILON = 1e-06
FLOOR = -1e30


def angles(positions, width):
    inverse = THETA ** (-jnp.arange(0, width, 2).astype(jnp.float32) / width)
    phase = positions.astype(jnp.float32)[:, None] * inverse[None, :]
    return (jnp.cos(phase), jnp.sin(phase))


def rotate(values, angle_cos, angle_sin):
    half = values.shape[-1] // 2
    first = values[..., :half].astype(jnp.float32)
    second = values[..., half:].astype(jnp.float32)
    turned = jnp.concatenate(
        [first * angle_cos - second * angle_sin, second * angle_cos + first * angle_sin], axis=-1
    )
    return turned.astype(jnp.bfloat16)


def norm_rows(values, gain):
    wide = values.astype(jnp.float32)
    scaled = wide * lax.rsqrt(jnp.mean(wide * wide, axis=-1, keepdims=True) + EPSILON)
    return (scaled * gain.astype(jnp.float32)).astype(jnp.bfloat16)


def split_query(query, heads, nope, angle_cos, angle_sin):
    shaped = query.reshape(query.shape[0], heads, -1)
    return (
        shaped[..., :nope],
        rotate(shaped[..., nope:], angle_cos[:, None, :], angle_sin[:, None, :]),
    )


def absorb(state, query_parts, key_nope, shared_block, values, offset, first, scale):
    query_nope, query_turned = query_parts
    scores = jnp.einsum("qhd,khd->hqk", query_nope, key_nope, preferred_element_type=jnp.float32)
    scores = scores + jnp.einsum(
        "qhd,kd->hqk", query_turned, shared_block, preferred_element_type=jnp.float32
    )
    scores = scores * scale
    query_pos = offset + jnp.arange(query_nope.shape[0], dtype=jnp.int32)
    key_pos = first + jnp.arange(key_nope.shape[0], dtype=jnp.int32)
    allowed = key_pos[None, :] <= query_pos[:, None]
    scores = jnp.where(allowed[None], scores, FLOOR)
    maximum, total, summed = state
    new_max = jnp.maximum(maximum, jnp.max(scores, axis=-1))
    weights = jnp.where(allowed[None], jnp.exp(scores - new_max[..., None]), 0.0)
    factor = jnp.exp(maximum - new_max)
    total = total * factor + jnp.sum(weights, axis=-1)
    summed = summed * factor[..., None] + jnp.einsum(
        "hqk,khd->hqd", weights.astype(jnp.bfloat16), values, preferred_element_type=jnp.float32
    )
    return (new_max, total, summed)


def finish(group_state):
    maximum, total, summed = group_state
    out = summed / total[..., None]
    return jnp.transpose(out, (1, 0, 2)).reshape(out.shape[1], -1).astype(jnp.bfloat16)


def on_device(
    resid,
    query_small,
    query_large,
    kv_latent,
    rope_key,
    kv_gain,
    up_key_small,
    up_value_small,
    up_key_large,
    up_value_large,
    out_weight,
    mix_gain,
    gate_weight,
    up_weight,
    down_weight,
):
    rows = kv_latent.shape[0]
    offset = lax.axis_index("sp") * rows
    last = offset + rows - 1
    positions = offset + jnp.arange(rows, dtype=jnp.int32)
    angle_cos, angle_sin = angles(positions, ROTARY)
    latent_normed = norm_rows(kv_latent, kv_gain)
    rotated_key = rotate(rope_key, angle_cos, angle_sin)
    heads_small = up_key_small.shape[1] // NOPE_SMALL
    heads_large = up_key_large.shape[1] // NOPE_LARGE
    small_parts = split_query(query_small, heads_small, NOPE_SMALL, angle_cos, angle_sin)
    large_parts = split_query(query_large, heads_large, NOPE_LARGE, angle_cos, angle_sin)
    scale_small = 1.0 / math.sqrt(NOPE_SMALL + ROTARY)
    scale_large = 1.0 / math.sqrt(NOPE_LARGE + ROTARY)

    def start_state(heads, width):
        return (
            jnp.full((heads, rows), FLOOR, jnp.float32),
            jnp.zeros((heads, rows), jnp.float32),
            jnp.zeros((heads, rows, width), jnp.float32),
        )

    initial = (start_state(heads_small, VALUE_SMALL), start_state(heads_large, VALUE_LARGE))

    def consume(state, keys_small, values_small, keys_large, values_large, shared_block, first):
        length = shared_block.shape[0]
        small = absorb(
            state[0],
            small_parts,
            keys_small.reshape(length, heads_small, NOPE_SMALL),
            shared_block,
            values_small.reshape(length, heads_small, VALUE_SMALL),
            offset,
            first,
            scale_small,
        )
        large = absorb(
            state[1],
            large_parts,
            keys_large.reshape(length, heads_large, NOPE_LARGE),
            shared_block,
            values_large.reshape(length, heads_large, VALUE_LARGE),
            offset,
            first,
            scale_large,
        )
        return (small, large)

    def expand(latent_block):
        return tuple(
            (
                jnp.dot(latent_block, matrix, preferred_element_type=jnp.float32).astype(
                    jnp.bfloat16
                )
                for matrix in (up_key_small, up_value_small, up_key_large, up_value_large)
            )
        )

    def from_latent(blocks):
        return expand(blocks[0]) + (blocks[1],)

    pieces = (
        lax.all_gather(latent_normed, "sp", axis=0, tiled=True),
        lax.all_gather(rotated_key, "sp", axis=0, tiled=True),
    )
    count = pieces[0].shape[0] // rows

    def step(index, inner):
        first = index * rows
        blocks = tuple((lax.dynamic_slice_in_dim(piece, index * rows, rows, 0) for piece in pieces))
        return lax.cond(
            first <= last,
            lambda held: consume(held, *from_latent(blocks), first),
            lambda held: held,
            inner,
        )

    state = lax.fori_loop(0, count, step, initial)
    attn_small = finish(state[0])
    attn_large = finish(state[1])
    border = HEADS_SMALL * VALUE_SMALL
    all_small, all_large = (
        lax.all_to_all(attn_small, "tp", split_axis=0, concat_axis=1, tiled=True),
        lax.all_to_all(attn_large, "tp", split_axis=0, concat_axis=1, tiled=True),
    )
    mixed = jnp.dot(all_small, out_weight[:border], preferred_element_type=jnp.float32)
    mixed = mixed + jnp.dot(all_large, out_weight[border:], preferred_element_type=jnp.float32)
    middle = (resid.astype(jnp.float32) + mixed).astype(jnp.bfloat16)
    mixer_in = norm_rows(middle, mix_gain)
    gate_whole, up_whole, down_whole = (
        lax.all_gather(gate_weight, "sp", axis=0, tiled=True),
        lax.all_gather(up_weight, "sp", axis=0, tiled=True),
        lax.all_gather(down_weight, "sp", axis=0, tiled=True),
    )
    piece = lax.all_gather(mixer_in, "tp", axis=0, tiled=True)
    gate = jnp.dot(piece, gate_whole, preferred_element_type=jnp.float32)
    upward = jnp.dot(piece, up_whole, preferred_element_type=jnp.float32)
    hidden = (jax.nn.silu(gate) * upward).astype(jnp.bfloat16)
    branch = lax.psum_scatter(
        lax.dot_general(
            hidden, down_whole, (((1,), (1,)), ((), ())), preferred_element_type=jnp.float32
        ).astype(jnp.bfloat16),
        "tp",
        scatter_dimension=0,
        tiled=True,
    ).astype(jnp.float32)
    return (middle.astype(jnp.float32) + branch).astype(jnp.bfloat16)


def solution(mesh):
    placed = (
        P(("sp", "tp"), None),
        P("sp", "tp"),
        P("sp", "tp"),
        P("sp", None),
        P("sp", None),
        P(),
        P(None, "tp"),
        P(None, "tp"),
        P(None, "tp"),
        P(None, "tp"),
        P(),
        P(),
        P("sp", "tp"),
        P("sp", "tp"),
        P("sp", "tp"),
    )
    return jax.shard_map(
        on_device, mesh=mesh, in_specs=placed, out_specs=P(("sp", "tp"), None), check_vma=False
    )
```

profile of v0, /device:TPU:0, one launch (start us, length us, event | category | flops | bytes accessed | tf_op | source)
XLA Modules:
  0.0 495.1 jit_solution(7308712939840525357)
XLA Ops:
  6.6 1.3 fusion.44
  7.9 0.7 convert_element_type.137
  8.5 1.9 fusion.46
  10.5 0.7 all-gather.10.cloned.1.call-update
  11.2 1.0 slice.49
  12.3 0.2 copy.33
  12.5 0.9 slice.46
  13.5 0.3 multiply_cosine_fusion
  13.8 0.9 fusion.56
  14.7 34.0 %all_gather.19 = bf16[6144,32]{0,1:T(8,128)(2,1)S(1)} all-gather(bf16[768,32]{0,1:T(8,128)(2,1)S(1)} %pad_maximum_fusion.2), channel_id=1, replica_groups=mesh['sp'=8,'tp'=4] {'sp'}, dimensions={0}, use_global_device_ids=true | all-gather | bytes 442368 | tf_op jit(solution)/shard_map/all_gather | solution.py:158
  48.8 26.8 %all-gather.6.cloned.1.call-done = bf16[6144,256]{1,0:T(8,128)(2,1)} async-done(((bf16[768,256]{1,0:T(8,128)(2,1)}), bf16[6144,256]{1,0:T(8,128)(2,1)}) %all-gather.6.cloned.1.call-update) | async-done | bytes 3145744 | tf_op jit(solution)/shard_map/all_gather | solution.py:157
  75.8 15.2 %while.23 = (s32[]{:T(128)}, f32[2,768]{1,0:T(2,128)S(1)}, f32[2,768]{1,0:T(2,128)S(1)}, f32[2,768,64]{1,2,0:T(8,128)S(1)}, f32[2,768]{1,0:T(2,128)S(1)}, /*inde...) while((s32[]{:T(128)}, f32[2,768]{1,0:T(2,128)S(1)}, ...), condition=%wide.region_8.9_spmd, body=%wide.region_1.8_spmd.sunk | while | flops 1384324608 | bytes 58503696 | solution.py:172
  75.8 14.9 %conditional.2 = ((f32[2,768]{1,0:T(2,128)S(1)}, f32[2,768]{1,0:T(2,128)S(1)}, f32[2,768,64]{1,2,0:T(8,128)S(1)}, f32[2,768]{1,0:T(2,128)S(1)}, f32[2,768]{1,0:T(2,128)S(1)}, /*index=5*/f32[2,768,128]{2,1,0:T(8,128)S(1)})) conditional(s32[]{:T(128)} %convert_element_type.251, (f32[2,768]{1,0:T(2,128)S(1)}, f32[2,768]{1,0:T(2,128)S(1)}, ...), branch_computations={%region_2.0_spmd, %region_3.7_spmd} | conditional | flops 1384324608 | bytes 58503288 | solution.py:165
  75.8 1.3 convolution_convert_fusion.1
  77.2 0.8 fusion.67
  78.0 0.4 broadcast_compare_fusion
  78.4 1.3 fusion.65
  79.7 1.3 convolution_convert_fusion.3
  81.0 0.8 fusion.66
  81.9 1.3 fusion.64
  83.2 1.8 fusion.7
  85.0 1.3 convolution_convert_fusion
  86.3 1.8 fusion.16
  88.1 1.3 convolution_convert_fusion.2
  89.4 1.3 fusion.19
  91.0 0.3 fusion.47
  91.3 0.4 copy.36
  91.7 1.0 convert_element_type.152
  92.7 3.5 all-to-all-start.1
  96.3 0.2 convert_element_type.149
  96.5 0.9 copy.34
  97.4 6.2 %all-to-all-done.1 = bf16[4,192,256]{2,1,0:T(8,128)(2,1)S(1)} async-done(((bf16[4,192,256]{2,1,0:T(8,128)(2,1)}), bf16[4,192,256]{2,1,0:T(8,128)(2,1)S(1)}, u32[]{:S(2)}, u32[]{:S(2)}) %all-to-all-start.1) | async-done | bytes 393248 | tf_op jit(solution)/shard_map/all_to_all | solution.py:178
  103.6 3.4 all-to-all-start
  107.0 0.2 all-gather.8.cloned.1.call-start
  107.2 3.2 fusion.38
  110.4 1.8 all-to-all-done
  112.2 2.5 multiply_reduce_fusion
  114.8 1.1 multiply_convert_fusion.1
  115.9 0.5 all-gather.12.cloned.1.call-update
  116.5 0.5 all-gather.14.cloned.1.call-update
  117.1 52.0 %all-gather.10.cloned.1.call-done = bf16[2048,1408]{1,0:T(8,128)(2,1)} async-done(((bf16[256,1408]{1,0:T(8,128)(2,1)}), bf16[2048,1408]{1,0:T(8,128)(2,1)}) %all-gather.10.cloned.1.call-update) | async-done | bytes 5767184 | tf_op jit(solution)/shard_map/all_gather | solution.py:185
  169.0 77.1 %all-gather.8.cloned.1.call-done = bf16[768,2048]{1,0:T(8,128)(2,1)} async-done(((bf16[192,2048]{1,0:T(8,128)(2,1)}), bf16[768,2048]{1,0:T(8,128)(2,1)}) %all-gather.8.cloned.1.call-update) | async-done | bytes 3145744 | tf_op jit(solution)/shard_map/all_gather | solution.py:189
  246.1 9.7 %fusion.68 = f32[768,1408]{1,0:T(8,128)} fusion(bf16[768,2048]{1,0:T(8,128)(2,1)} %all-gather.8.cloned.1.call-done, bf16[2048,1408]{1,0:T(8,128)(2,1)} %all-gather.10.cloned.1.call-done), kind=kOutput, calls=%fused_computation.108 | convolution fusion | flops 4429185024 | bytes 13238272 | tf_op jit(solution)/shard_map/dot_general | solution.py:190
  255.8 84.7 %all-gather.12.cloned.1.call-done = bf16[2048,1408]{1,0:T(8,128)(2,1)} async-done(((bf16[256,1408]{1,0:T(8,128)(2,1)}), bf16[2048,1408]{1,0:T(8,128)(2,1)}) %all-gather.12.cloned.1.call-update) | async-done | bytes 5767184 | tf_op jit(solution)/shard_map/all_gather | solution.py:186
  340.5 92.6 %all-gather.14.cloned.1.call-done = bf16[2048,1408]{1,0:T(8,128)(2,1)} async-done(((bf16[256,1408]{1,0:T(8,128)(2,1)}), bf16[2048,1408]{1,0:T(8,128)(2,1)}) %all-gather.14.cloned.1.call-update) | async-done | bytes 5767184 | tf_op jit(solution)/shard_map/all_gather | solution.py:187
  433.1 16.7 %convolution_convert_fusion.4 = bf16[768,2048]{1,0:T(8,128)(2,1)} fusion(bf16[2048,1408]{1,0:T(8,128)(2,1)} %all-gather.14.cloned.1.call-done, f32[768,1408]{1,0:T(8,128)} %fusion.68, bf16[768,2048]{1,0:T(8,128)(2,1)} %all-gather.8.cloned.1.call-done, bf16[2048,1408]{1,0:T(8,128)(2,1)} %all-gather.12.cloned.1.call-done), kind=kOutput, calls=%fused_computation.50 | convolution fusion | flops 8866430976 | bytes 22151168 | tf_op jit(solution)/shard_map/dot_general | solution.py:194
  449.8 36.2 %reduce-scatter.2.cloned.1.call-done = bf16[192,2048]{1,0:T(8,128)(2,1)} async-done(((bf16[768,2048]{1,0:T(8,128)(2,1)}), bf16[192,2048]{1,0:T(8,128)(2,1)}) %reduce-scatter.2.cloned.1.call-update) | async-done | bytes 786448 | tf_op jit(solution)/shard_map/reduce_scatter | solution.py:193
  486.0 2.2 add_convert_fusion
  (49 shorter events, 0.6 us)
Async XLA Ops:
  6.5 6.9 %copy-start.4 = (bf16[768,32]{0,1:T(8,128)(2,1)S(1)}, bf16[768,32]{0,1:T(8,128)(2,1)}, u32[]{:S(2)}) copy-start(bf16[768,32]{0,1:T(8,128)(2,1)} %param.23) | copy-start | bytes 147460
  6.5 69.2 %copy-start.2 = (bf16[256,128]{1,0:T(8,128)(2,1)S(1)}, bf16[256,128]{1,0:T(8,128)(2,1)}, u32[]{:S(2)}) copy-start(bf16[256,128]{1,0:T(8,128)(2,1)} %param.25) | copy-start | bytes 196612
  6.5 69.2 %copy-start.3 = (bf16[256,128]{1,0:T(8,128)(2,1)S(1)}, bf16[256,128]{1,0:T(8,128)(2,1)}, u32[]{:S(2)}) copy-start(bf16[256,128]{1,0:T(8,128)(2,1)} %param.26) | copy-start | bytes 196612
  6.5 69.2 %copy-start = (bf16[256,256]{1,0:T(8,128)(2,1)S(1)}, bf16[256,256]{1,0:T(8,128)(2,1)}, u32[]{:S(2)}) copy-start(bf16[256,256]{1,0:T(8,128)(2,1)} %param.27) | copy-start | bytes 393220
  6.5 69.2 %copy-start.1 = (bf16[256,256]{1,0:T(8,128)(2,1)S(1)}, bf16[256,256]{1,0:T(8,128)(2,1)}, u32[]{:S(2)}) copy-start(bf16[256,256]{1,0:T(8,128)(2,1)} %param.28) | copy-start | bytes 393220
  6.5 69.0 %all-gather.6.cloned.1.call-start = ((), (), s32[]{:S(2)}) async-start(), calls=%async_computation.3 | async-start | bytes 3538944 | tf_op jit(solution)/shard_map/all_gather | solution.py:157
  10.5 158.6 %all-gather.10.cloned.1.call-start = ((), (), s32[]{:S(2)}) async-start(), calls=%async_computation.5 | async-start | bytes 6488064 | tf_op jit(solution)/shard_map/all_gather | solution.py:185
  75.8 20.4 %copy-start.5 = (bf16[2048]{0:T(1024)(128)(2,1)S(1)}, bf16[2048]{0:T(1024)(128)(2,1)}, u32[]{:S(2)}) copy-start(bf16[2048]{0:T(1024)(128)(2,1)} %param.30) | copy-start | bytes 12292
  92.7 10.8 %all-to-all-start.1 = ((bf16[4,192,256]{2,1,0:T(8,128)(2,1)}), bf16[4,192,256]{2,1,0:T(8,128)(2,1)S(1)}, u32[]{:S(2)}, u32[]{:S(2)}) async-start(bf16[4,192,256]{2,1,0:T(8,128)(2,1)} %convert_element_type.152), calls=%async_computation.1 | async-start | bytes 786432 | tf_op jit(solution)/shard_map/all_to_all | solution.py:178
  103.6 8.6 %all-to-all-start = ((bf16[4,192,128]{2,1,0:T(8,128)(2,1)}), bf16[4,192,128]{2,1,0:T(8,128)(2,1)S(1)}, u32[]{:S(2)}, u32[]{:S(2)}) async-start(bf16[4,192,128]{2,1,0:T(8,128)(2,1)} %copy.34), calls=%async_computation | async-start | bytes 393216 | tf_op jit(solution)/shard_map/all_to_all | solution.py:177
  107.0 139.2 %all-gather.8.cloned.1.call-start = ((), (), s32[]{:S(2)}) async-start(), calls=%async_computation.4 | async-start | bytes 3932160 | tf_op jit(solution)/shard_map/all_gather | solution.py:189
  115.9 224.7 %all-gather.12.cloned.1.call-start = ((), (), s32[]{:S(2)}) async-start(), calls=%async_computation.6 | async-start | bytes 6488064 | tf_op jit(solution)/shard_map/all_gather | solution.py:186
  116.4 316.6 %all-gather.14.cloned.1.call-start = ((), (), s32[]{:S(2)}) async-start(), calls=%async_computation.7 | async-start | bytes 6488064 | tf_op jit(solution)/shard_map/all_gather | solution.py:187
  117.0 369.0 %reduce-scatter.2.cloned.1.call-start = ((), (), s32[]{:S(2)}) async-start(), calls=%async_computation.8 | async-start | bytes 3932160 | tf_op jit(solution)/shard_map/reduce_scatter | solution.py:193
Sparse Core Ops, SparseCore 0:
  10.6 64.9 all-gather.5
  77.8 91.2 all-gather.9
  170.6 75.4 all-gather.7
  248.2 92.3 all-gather.11
  342.6 90.4 all-gather.13
  449.9 36.0 reduce-scatter.1
where the time goes:
time: 497 us; the launch traced here: 495 us
  waiting for transfers between devices  379 us (76%)
  matrix products  44.7 us (9%)
  blocking collectives  34 us (7%)
  between operations  13.7 us (3%)
  other arithmetic  10.9 us (2%)
  starting transfers between devices  7.25 us (1%)
    all_gather x1, waiting for transfers between devices, on_device(): lax.all_gather(down_weight, 'sp', axis=0, tiled=True)  92.6 us
    all_gather x1, waiting for transfers between devices, on_device(): lax.all_gather(up_weight, 'sp', axis=0, tiled=True)  84.7 us
    all_gather x1, waiting for transfers between devices, on_device(): piece = lax.all_gather(mixer_in, 'tp', axis=0, tiled=True)  77.1 us
    all_gather x1, waiting for transfers between devices, on_device(): lax.all_gather(gate_weight, 'sp', axis=0, tiled=True)  52 us
    reduce_scatter x1, waiting for transfers between devices, on_device(): lax.psum_scatter(lax.dot_general(hidden, down_whole, (((1,), (1,)), ((),...  36.2 us
    all_gather x1, blocking collectives, on_device(): lax.all_gather(rotated_key, 'sp', axis=0, tiled=True)  34 us
    all_gather x1, waiting for transfers between devices, on_device(): lax.all_gather(latent_normed, 'sp', axis=0, tiled=True)  26.8 us
    dot_general x1, matrix products, on_device(): lax.dot_general(hidden, down_whole, (((1,), (1,)), ((), ())), preferred_e...  16.7 us
  transfers between devices with their start and end apart: 8, of which 8 were waited for; matrix products, arithmetic and copies ran while one was open for 8% of the time, Pallas kernels for 0%

commit v1 on v0

v1 whole, which is shorter than its diff:
```python
import functools
import math

import jax
import jax.numpy as jnp
from jax import lax
from jax.experimental import pallas as pl
from jax.experimental.pallas import tpu as pltpu
from jax.sharding import PartitionSpec as P

HEADS_SMALL = 8
NOPE_SMALL = 64
NOPE_LARGE = 128
VALUE_SMALL = 64
VALUE_LARGE = 128
ROTARY = 32


THETA = 10000.0
EPSILON = 1e-06
FLOOR = -1e30


def angles(positions, width):
    inverse = THETA ** (-jnp.arange(0, width, 2).astype(jnp.float32) / width)
    phase = positions.astype(jnp.float32)[:, None] * inverse[None, :]
    return (jnp.cos(phase), jnp.sin(phase))


def rotate(values, angle_cos, angle_sin):
    half = values.shape[-1] // 2
    first = values[..., :half].astype(jnp.float32)
    second = values[..., half:].astype(jnp.float32)
    turned = jnp.concatenate(
        [first * angle_cos - second * angle_sin, second * angle_cos + first * angle_sin], axis=-1
    )
    return turned.astype(jnp.bfloat16)


def norm_rows(values, gain):
    wide = values.astype(jnp.float32)
    scaled = wide * lax.rsqrt(jnp.mean(wide * wide, axis=-1, keepdims=True) + EPSILON)
    return (scaled * gain.astype(jnp.float32)).astype(jnp.bfloat16)


LOG2E = math.log2(math.e)
TILE = 256
PAD = 16


def ring_place(index, count):
    return jnp.where(index % 2 == 0, index // 2, count - 1 - index // 2)


def ring_index(place, count):
    place = (place + 2 * count) % count
    return jnp.where(place < count // 2, 2 * place, 2 * (count - 1 - place) + 1)


def attend_and_gather(count, shapes, *refs):
    (shared, expand_key, expand_value, query_small, query_large, gate, up) = refs[:7]
    out, gate_all, up_all = refs[7:10]
    maxima, sums, send_sem, recv_sem, own_sem = refs[10:]
    me = lax.axis_index("sp")
    place = ring_place(me, count)
    right, left = ring_index(place + 1, count), ring_index(place - 1, count)
    weights, wholes = (gate, up), (gate_all, up_all)
    depth = gate.shape[0]
    half = depth // 2
    last = count // 2

    barrier = pltpu.get_barrier_semaphore()
    for side in (right, left):
        pl.semaphore_signal(
            barrier, inc=1, device_id={"sp": side}, device_id_type=pl.DeviceIdType.MESH
        )
    pl.semaphore_wait(barrier, 2)

    def hop(way, step, which):
        origin = ring_index(place - (step - 1) if way == 0 else place + (step - 1), count)
        source = weights[which] if step == 1 else wholes[which].at[origin]
        target = wholes[which].at[origin]
        if step == last:
            span = pl.ds(way * half, half)
            source, target = source.at[span], target.at[span]
        return pltpu.make_async_remote_copy(
            src_ref=source,
            dst_ref=target,
            send_sem=send_sem.at[way, step - 1, which],
            recv_sem=recv_sem.at[way, step - 1, which],
            device_id={"sp": right if way == 0 else left},
            device_id_type=pl.DeviceIdType.MESH,
        )

    def own(which):
        return pltpu.make_async_copy(weights[which], wholes[which].at[me], own_sem.at[which])

    for which in range(2):
        for way in range(2):
            hop(way, 1, which).start()
    for which in range(2):
        own(which).start()

    events = [(step, which) for step in range(1, last) for which in range(2)]

    def forward(step, which):
        for way in range(2):
            hop(way, step, which).wait_recv()
            hop(way, step + 1, which).start()

    maxima[...] = jnp.full(maxima.shape, FLOOR, jnp.float32)
    sums[...] = jnp.zeros(sums.shape, jnp.float32)
    rows = query_small.shape[-1]

    def block(index, diagonal):
        start = pl.multiple_of(index * rows, rows)
        latent = shared[pl.ds(start, rows), :]
        for head, (group, inner, nope, wide, key_at, width, value_at, sum_at, out_at) in enumerate(shapes):
            key = jnp.dot(
                latent, expand_key[:, key_at : key_at + wide], preferred_element_type=jnp.float32
            ).astype(jnp.bfloat16)
            value = lax.dot_general(
                expand_value[value_at : value_at + width, :],
                latent,
                (((1,), (1,)), ((), ())),
                preferred_element_type=jnp.float32,
            ).astype(jnp.bfloat16)
            value = jnp.concatenate([value, jnp.ones((PAD, rows), jnp.bfloat16)], axis=0)
            scale = LOG2E / math.sqrt(nope + ROTARY)
            query = query_small if group == 0 else query_large
            for tile in range(rows // TILE):
                columns = slice(tile * TILE, (tile + 1) * TILE)
                length = (tile + 1) * TILE if diagonal else rows
                scores = jnp.dot(
                    key[:length], query[inner, :, columns], preferred_element_type=jnp.float32
                )
                if diagonal:
                    key_pos = lax.broadcasted_iota(jnp.int32, scores.shape, 0)
                    query_pos = lax.broadcasted_iota(jnp.int32, scores.shape, 1) + tile * TILE
                    scores = jnp.where(key_pos <= query_pos, scores, FLOOR)
                old = maxima[head, :, columns]
                new = jnp.maximum(old, jnp.max(scores, axis=0, keepdims=True))
                weight = jnp.exp2((scores - new) * scale).astype(jnp.bfloat16)
                factor = jnp.exp2((old - new) * scale)
                place_of = slice(sum_at, sum_at + width + PAD)
                total = sums[place_of, columns] * factor + jnp.dot(
                    value[:, :length], weight, preferred_element_type=jnp.float32
                )
                if diagonal:
                    out[out_at : out_at + width, columns] = (
                        total[:width] / total[width : width + 1]
                    ).astype(jnp.bfloat16)
                else:
                    maxima[head, :, columns] = new
                    sums[place_of, columns] = total

    def step_of(index, carry):
        for number, event in enumerate(events):

            @pl.when(index == 2 * number + 2)
            def _():
                forward(*event)

        block(index, False)
        return carry

    lax.fori_loop(0, me, step_of, 0)
    block(me, True)
    for number, event in enumerate(events):

        @pl.when(me <= 2 * number + 2)
        def _():
            forward(*event)

    for which in range(2):
        own(which).wait()
        for way in range(2):
            hop(way, last, which).wait_recv()
            for step in range(1, last + 1):
                hop(way, step, which).wait_send()


def on_device(
    count,
    resid,
    query_small,
    query_large,
    kv_latent,
    rope_key,
    kv_gain,
    up_key_small,
    up_value_small,
    up_key_large,
    up_value_large,
    out_weight,
    mix_gain,
    gate_weight,
    up_weight,
    down_weight,
):
    rows, latent_size = kv_latent.shape
    offset = lax.axis_index("sp") * rows
    positions = offset + jnp.arange(rows, dtype=jnp.int32)
    angle_cos, angle_sin = angles(positions, ROTARY)
    shared = jnp.concatenate(
        [norm_rows(kv_latent, kv_gain), rotate(rope_key, angle_cos, angle_sin)], axis=1
    )
    shared = jnp.pad(lax.all_gather(shared, "sp", axis=0, tiled=True), ((0, 0), (0, 128 - ROTARY)))
    resid, down_weight, shared = lax.optimization_barrier((resid, down_weight, shared))
    resid_all = lax.all_gather(resid, "tp", axis=0, tiled=True)
    down_whole = lax.all_gather(down_weight, "sp", axis=0, tiled=True)

    shapes = []
    queries, keys, values = [], [], []
    key_at = value_at = sum_at = 0
    for group, (query, up_key, up_value, nope, width) in enumerate(
        (
            (query_small, up_key_small, up_value_small, NOPE_SMALL, VALUE_SMALL),
            (query_large, up_key_large, up_value_large, NOPE_LARGE, VALUE_LARGE),
        )
    ):
        heads = up_key.shape[1] // nope
        wide = nope + ROTARY
        padded = -(-wide // 128) * 128
        shaped = query.reshape(rows, heads, wide)
        turned = rotate(shaped[..., nope:], angle_cos[:, None, :], angle_sin[:, None, :])
        full = jnp.concatenate([shaped[..., :nope], turned], axis=-1)
        full = jnp.pad(full, ((0, 0), (0, 0), (0, padded - wide)))
        queries.append(jnp.transpose(full, (1, 2, 0)))
        rotary_part = jnp.eye(128, padded, k=nope, dtype=jnp.bfloat16)
        rotary_part = jnp.where(jnp.arange(128)[:, None] < ROTARY, rotary_part, 0)
        for head in range(heads):
            part = jnp.pad(up_key[:, head * nope : (head + 1) * nope], ((0, 0), (0, padded - nope)))
            keys.append(jnp.concatenate([part, rotary_part.astype(jnp.bfloat16)], axis=0))
            shapes.append((group, head, nope, padded, key_at, width, value_at, sum_at, value_at))
            key_at += padded
            value_at += width
            sum_at += width + PAD
        values.append(jnp.pad(jnp.transpose(up_value), ((0, 0), (0, 128))))
    expand_key = jnp.concatenate(keys, axis=1)
    expand_value = jnp.concatenate(values, axis=0)
    depth, hidden_size = gate_weight.shape
    vmem = pl.BlockSpec(memory_space=pltpu.VMEM)
    hbm = pl.BlockSpec(memory_space=pl.ANY)
    whole = jax.ShapeDtypeStruct((count, depth, hidden_size), jnp.bfloat16)
    attn, gate_whole, up_whole = pl.pallas_call(
        functools.partial(attend_and_gather, count, tuple(shapes)),
        out_shape=(jax.ShapeDtypeStruct((value_at, rows), jnp.bfloat16), whole, whole),
        in_specs=[vmem] * 5 + [hbm] * 2,
        out_specs=(vmem, hbm, hbm),
        scratch_shapes=[
            pltpu.VMEM((len(shapes), 1, rows), jnp.float32),
            pltpu.VMEM((sum_at, rows), jnp.float32),
            pltpu.SemaphoreType.DMA((2, count // 2, 2)),
            pltpu.SemaphoreType.DMA((2, count // 2, 2)),
            pltpu.SemaphoreType.DMA((2,)),
        ],
        compiler_params=pltpu.CompilerParams(
            collective_id=0, has_side_effects=True, vmem_limit_bytes=50 * 2**20
        ),
        cost_estimate=pl.CostEstimate(
            flops=10**11, bytes_accessed=3 * 10**7, transcendentals=2 * 10**7
        ),
    )(shared, expand_key, expand_value, queries[0], queries[1], gate_weight, up_weight)
    gate_whole = gate_whole.reshape(count * depth, hidden_size)
    up_whole = up_whole.reshape(count * depth, hidden_size)
    border_device = up_value_small.shape[1]
    attn_all = lax.all_gather(attn, "tp", axis=0)
    attn_small = attn_all[:, :border_device].reshape(-1, rows)
    attn_large = attn_all[:, border_device:].reshape(-1, rows)
    border = HEADS_SMALL * VALUE_SMALL
    over_first = (((0,), (0,)), ((), ()))
    mixed = lax.dot_general(
        attn_small, out_weight[:border], over_first, preferred_element_type=jnp.float32
    )
    mixed = mixed + lax.dot_general(
        attn_large, out_weight[border:], over_first, preferred_element_type=jnp.float32
    )
    middle_all = (resid_all.astype(jnp.float32) + mixed).astype(jnp.bfloat16)
    mixer_in = norm_rows(middle_all, mix_gain)
    gate = jnp.dot(mixer_in, gate_whole, preferred_element_type=jnp.float32)
    upward = jnp.dot(mixer_in, up_whole, preferred_element_type=jnp.float32)
    hidden = (jax.nn.silu(gate) * upward).astype(jnp.bfloat16)
    branch = lax.psum_scatter(
        lax.dot_general(
            hidden, down_whole, (((1,), (1,)), ((), ())), preferred_element_type=jnp.float32
        ).astype(jnp.bfloat16),
        "tp",
        scatter_dimension=0,
        tiled=True,
    ).astype(jnp.float32)
    middle = lax.dynamic_slice_in_dim(
        middle_all, lax.axis_index("tp") * resid.shape[0], resid.shape[0], 0
    )
    return (middle.astype(jnp.float32) + branch).astype(jnp.bfloat16)


def solution(mesh):
    placed = (
        P(("sp", "tp"), None),
        P("sp", "tp"),
        P("sp", "tp"),
        P("sp", None),
        P("sp", None),
        P(),
        P(None, "tp"),
        P(None, "tp"),
        P(None, "tp"),
        P(None, "tp"),
        P(),
        P(),
        P("sp", "tp"),
        P("sp", "tp"),
        P("sp", "tp"),
    )
    return jax.shard_map(
        functools.partial(on_device, mesh.shape["sp"]), mesh=mesh, in_specs=placed, out_specs=P(("sp", "tp"), None), check_vma=False
    )
```

time: 497 us -> 425 us (0.86)
  waiting for transfers between devices: 379 us -> 236 us
  Pallas kernels: 0 us -> 113 us
  blocking collectives: 34 us -> 0 us
  starting transfers between devices: 7.25 us -> 0.16 us
  local copies, waits for them, and re-layouts: 4.89 us -> 10.4 us
    all_gather x5 -> x4, waiting for transfers between devices: 333 us -> 199 us  [the longest x1 80.8 us: on_device(): lax.all_gather(shared, 'sp', axis=0, tiled=True)]
    pallas_call x0 -> x1, Pallas kernels: none -> 113 us  [on_device(): pl.pallas_call(functools.partial(attend_and_gather, count, tuple(shapes))...]
    all_gather x1 -> x0, blocking collectives: 34 us -> none  [on_device(): lax.all_gather(rotated_key, 'sp', axis=0, tiled=True)]
    all_to_all x2 -> x0, waiting for transfers between devices: 7.98 us -> none  [the longest x1 6.17 us: on_device(): lax.all_to_all(attn_large, 'tp', split_axis=0, concat_axis=1, tiled=True)]
    all_to_all x2 -> x0, starting transfers between devices: 6.83 us -> none  [the longest x1 3.46 us: on_device(): lax.all_to_all(attn_large, 'tp', split_axis=0, concat_axis=1, tiled=True)]
    pad x0 -> x1, local copies, waits for them, and re-layouts: none -> 4.99 us  [on_device(): jnp.pad(lax.all_gather(shared, 'sp', axis=0, tiled=True), ((0, 0), (0, 12...]
    dot_general x13 -> x3, matrix products: 27.9 us -> 24.2 us  [the longest x1 9.86 us: on_device(): gate = jnp.dot(mixer_in, gate_whole, preferred_element_type=jnp.float32)]
  transfers between devices with their start and end apart: 8 -> 5, of which waited for: 8 -> 5; matrix products, arithmetic and copies ran while one was open for 8% -> 7% of each run, Pallas kernels for 0% -> 0%
where the time goes in v1:
time: 425 us; the launch traced here: 424 us
  waiting for transfers between devices  236 us (56%)
  Pallas kernels  113 us (27%)
  matrix products  41.1 us (10%)
  between operations  13.5 us (3%)
  local copies, waits for them, and re-layouts  10.4 us (2%)
  other arithmetic  9.54 us (2%)
    pallas_call x1, Pallas kernels, on_device(): pl.pallas_call(functools.partial(attend_and_gather, count, tuple(shapes))...  113 us
    all_gather x1, waiting for transfers between devices, on_device(): lax.all_gather(shared, 'sp', axis=0, tiled=True)  80.8 us
    all_gather x1, waiting for transfers between devices, on_device(): down_whole = lax.all_gather(down_weight, 'sp', axis=0, tiled=True)  76.1 us
    reduce_scatter x1, waiting for transfers between devices, on_device(): lax.psum_scatter(lax.dot_general(hidden, down_whole, (((1,), (1,)), ((),...  36.2 us
    all_gather x1, waiting for transfers between devices, on_device(): attn_all = lax.all_gather(attn, 'tp', axis=0)  22 us
    all_gather x1, waiting for transfers between devices, on_device(): resid_all = lax.all_gather(resid, 'tp', axis=0, tiled=True)  19.8 us
    dot_general x1, matrix products, on_device(): lax.dot_general(hidden, down_whole, (((1,), (1,)), ((), ())), preferred_e...  17 us
    dot_general x1, matrix products, on_device(): gate = jnp.dot(mixer_in, gate_whole, preferred_element_type=jnp.float32)  9.86 us
  transfers between devices with their start and end apart: 5, of which 5 were waited for; matrix products, arithmetic and copies ran while one was open for 7% of the time, Pallas kernels for 0%

profile of v1, /device:TPU:0, one launch (start us, length us, event | category | flops | bytes accessed | tf_op | source)
XLA Modules:
  0.0 424.2 jit_solution(6559293799328714365)
XLA Ops:
  6.5 0.8 slice_convert_fusion
  7.3 0.2 copy.22
  7.5 0.0 copy-start.2
  7.5 0.2 copy.23
  7.7 1.2 fusion.21
  8.9 0.0 copy-start.4
  8.9 0.7 convert_element_type.105
  9.6 1.2 fusion.23
  10.8 0.0 copy-start.7
  10.8 0.0 copy-start.8
  10.8 1.8 multiply_cosine_fusion
  12.6 0.9 pad_maximum_fusion
  13.5 0.0 all-gather.6.cloned.1.call-update
  13.6 0.0 all-gather.12.cloned.1.call-start
  13.6 0.1 copy.27
  13.7 0.1 copy.28
  14.0 0.1 slice.54
  14.1 0.1 copy.26
  14.2 0.1 copy.25
  14.4 0.1 fusion.51
  14.5 0.1 fusion.26.refs_4_
  14.5 0.1 fusion.56
  14.6 0.1 fusion.54
  14.8 0.1 fusion.31.refs_1_
  14.9 0.0 copy-start
  14.9 0.0 copy-start.1
  14.9 80.8 %all-gather.6.cloned.1.call-done = bf16[6144,288]{1,0:T(8,128)(2,1)} async-done(((bf16[768,288]{1,0:T(8,128)(2,1)}), bf16[6144,288]{1,0:T(8,128)(2,1)}) %all-gather.6.cloned.1.call-update) | async-done | bytes 3538960 | tf_op jit(solution)/shard_map/all_gather | solution.py:208
  95.8 5.0 %pad.34.refs_0_ = bf16[6144,384]{1,0:T(8,128)(2,1)} pad(bf16[6144,288]{1,0:T(8,128)(2,1)} %all-gather.6.cloned.1.call-done, bf16[]{:T(256)} %constant.36.clone.1), padding=0_0x0_96 | pad | bytes 8257538 | tf_op jit(solution)/shard_map/jit(_pad)/pad | solution.py:208
  100.8 113.4 %shard_map.145 = (bf16[384,768]{1,0:T(8,128)(2,1)}, bf16[8,256,1408]{2,1,0:T(8,128)(2,1)}, bf16[8,256,1408]{2,1,0:T(8,128)(2,1)}) custom-call(bf16[6144,384]{1,0:T(8,128)(2,1)} %pad.34.refs_0_, bf16[384,768]{1,0:T(8,128)(2,1)S(1)} %fusion.31.refs_1_, bf16[384,384]{1,0:T(8,128)(2,1)S(1)} %fusion.44.refs_2_, bf16[2,128,768]{2,1,0:T(8,128)(2,1)S(1)} %fusion.43.refs_3_, ...), custom_call_target="tpu_custom_call" | custom-call | flops 99999997952 | bytes 30000000 | tf_op jit(solution)/shard_map/pallas_call | solution.py:246
  214.1 0.0 all-gather.12.cloned.1.call-update
  214.2 0.0 all-gather.8.cloned.1.call-start
  214.2 0.7 all-gather.8.cloned.1.call-update
  214.9 0.0 all-gather.10.cloned.1.call-start
  214.9 0.5 all-gather.10.cloned.1.call-update
  215.5 0.0 reduce-scatter.2.cloned.1.call-start
  215.5 22.0 %all-gather.12.cloned.1.call-done = bf16[1536,768]{1,0:T(8,128)(2,1)} async-done(((bf16[384,768]{1,0:T(8,128)(2,1)}), bf16[1536,768]{1,0:T(8,128)(2,1)}) %all-gather.12.cloned.1.call-update) | async-done | bytes 2359312 | tf_op jit(solution)/shard_map/all_gather | solution.py:268
  237.5 1.5 slice.73
  239.0 1.2 slice.72
  240.2 7.6 %fusion.3 = f32[768,2048]{1,0:T(8,128)} fusion(bf16[1024,768]{1,0:T(8,128)(2,1)S(1)} %bitcast.18, bf16[1536,2048]{1,0:T(8,128)(2,1)} %param.25), kind=kOutput, calls=%fused_computation.7 | convolution fusion | flops 3221225472 | bytes 12058624 | tf_op jit(solution)/shard_map/dot_general | solution.py:276
  247.8 19.8 %all-gather.8.cloned.1.call-done = bf16[768,2048]{1,0:T(8,128)(2,1)} async-done(((bf16[192,2048]{1,0:T(8,128)(2,1)}), bf16[768,2048]{1,0:T(8,128)(2,1)}) %all-gather.8.cloned.1.call-update) | async-done | bytes 3145744 | tf_op jit(solution)/shard_map/all_gather | solution.py:210
  267.6 6.7 %fusion = (f32[768]{0:T(1024)S(1)}, bf16[768,2048]{1,0:T(8,128)(2,1)S(1)}) fusion(f32[768,2048]{1,0:T(8,128)} %fusion.3, bf16[512,768]{1,0:T(8,128)(2,1)S(1)} %bitcast.21, bf16[1536,2048]{1,0:T(8,128)(2,1)} %param.25, bf16[768,2048]{1,0:T(8,128)(2,1)} %all-gather.8.cloned.1.call-done), kind=kOutput, calls=%fused_computation.2 | convolution fusion | flops 1621622016 | bytes 15469568 | tf_op jit(solution)/shard_map/dot_general | solution.py:273
  274.4 1.7 copy-done.6
  276.1 9.9 %fusion.17 = f32[768,1408]{1,0:T(8,128)} fusion(bf16[2048,1408]{1,0:T(8,128)(2,1)} %bitcast.29, bf16[768,2048]{1,0:T(8,128)(2,1)S(1)} %get-tuple-element.32, f32[2048]{0:T(1024)S(1)} %convert_element_type.121, f32[768]{0:T(1024)S(1)} %add_rsqrt_fusion), kind=kOutput, calls=%fused_computation.29 | convolution fusion | flops 4435476480 | bytes 13249536 | tf_op jit(solution)/shard_map/dot_general | solution.py:281
  285.9 76.1 %all-gather.10.cloned.1.call-done = bf16[2048,1408]{1,0:T(8,128)(2,1)} async-done(((bf16[256,1408]{1,0:T(8,128)(2,1)}), bf16[2048,1408]{1,0:T(8,128)(2,1)}) %all-gather.10.cloned.1.call-update) | async-done | bytes 5767184 | tf_op jit(solution)/shard_map/all_gather | solution.py:211
  362.0 17.0 %convolution_convert_fusion = bf16[768,2048]{1,0:T(8,128)(2,1)} fusion(bf16[2048,1408]{1,0:T(8,128)(2,1)} %all-gather.10.cloned.1.call-done, f32[768,1408]{1,0:T(8,128)} %fusion.17, bf16[2048,1408]{1,0:T(8,128)(2,1)} %bitcast.28, bf16[768,2048]{1,0:T(8,128)(2,1)} %copy-done.6, f32[2048]{0:T(1024)S(1)} %convert_element_type.121, f32[768]{0:T(1024)S(1)} %add_rsqrt_fusion), kind=kOutput, calls=%fused_computation.9 | convolution fusion | flops 8872722432 | bytes 22162432 | tf_op jit(solution)/shard_map/dot_general | solution.py:285
  378.9 0.0 reduce-scatter.2.cloned.1.call-update
  379.0 36.2 %reduce-scatter.2.cloned.1.call-done = bf16[192,2048]{1,0:T(8,128)(2,1)} async-done(((bf16[768,2048]{1,0:T(8,128)(2,1)}), bf16[192,2048]{1,0:T(8,128)(2,1)}) %reduce-scatter.2.cloned.1.call-update) | async-done | bytes 786448 | tf_op jit(solution)/shard_map/reduce_scatter | solution.py:284
  415.2 2.5 add_convert_fusion.1
  (34 shorter events, 0.2 us)
Async XLA Ops:
  6.5 89.2 %all-gather.6.cloned.1.call-start = ((), (), s32[]{:S(2)}) async-start(), calls=%async_computation.1 | async-start | bytes 5308416 | tf_op jit(solution)/shard_map/all_gather | solution.py:208
  7.5 6.4 %copy-start.2 = (bf16[768,320]{0,1:T(8,128)(2,1)S(1)}, bf16[768,320]{0,1:T(8,128)(2,1)}, u32[]{:S(2)}) copy-start(bf16[768,320]{0,1:T(8,128)(2,1)} %param.17) | copy-start | bytes 1474564
  8.9 5.1 %copy-start.4 = (bf16[768,192]{0,1:T(8,128)(2,1)S(1)}, bf16[768,192]{0,1:T(8,128)(2,1)}, u32[]{:S(2)}) copy-start(bf16[768,192]{0,1:T(8,128)(2,1)} %param.16) | copy-start | bytes 884740
  9.6 4.4 %copy-start.5 = (bf16[256,128]{1,0:T(8,128)(2,1)S(1)}, bf16[256,128]{1,0:T(8,128)(2,1)}, u32[]{:S(2)}) copy-start(bf16[256,128]{1,0:T(8,128)(2,1)} %param.21) | copy-start | bytes 196612
  10.8 3.3 copy-start.7
  10.8 3.4 copy-start.8
  13.5 1.2 copy-start.11
  13.5 1.3 copy-start.3
  13.5 1.3 copy-start.10
  13.5 1.3 slice-start
  13.6 223.9 %all-gather.12.cloned.1.call-start = ((), (), s32[]{:S(2)}) async-start(), calls=%async_computation.5 | async-start | bytes 2949120 | tf_op jit(solution)/shard_map/all_gather | solution.py:268
  14.9 85.9 %copy-start = (bf16[256,1408]{1,0:T(8,128)(2,1)S(1)}, bf16[256,1408]{1,0:T(8,128)(2,1)}, u32[]{:S(2)}) copy-start(bf16[256,1408]{1,0:T(8,128)(2,1)} %refs_5_.1) | copy-start | bytes 2162692
  14.9 85.9 %copy-start.1 = (bf16[256,1408]{1,0:T(8,128)(2,1)S(1)}, bf16[256,1408]{1,0:T(8,128)(2,1)}, u32[]{:S(2)}) copy-start(bf16[256,1408]{1,0:T(8,128)(2,1)} %refs_6_.1) | copy-start | bytes 2162692
  100.7 114.8 %copy-start.9 = (bf16[2048]{0:T(1024)(128)(2,1)S(1)}, bf16[2048]{0:T(1024)(128)(2,1)}, u32[]{:S(2)}) copy-start(bf16[2048]{0:T(1024)(128)(2,1)} %param.26) | copy-start | bytes 12292
  214.2 53.4 %all-gather.8.cloned.1.call-start = ((), (), s32[]{:S(2)}) async-start(), calls=%async_computation.2 | async-start | bytes 3932160 | tf_op jit(solution)/shard_map/all_gather | solution.py:210
  214.9 147.1 %all-gather.10.cloned.1.call-start = ((), (), s32[]{:S(2)}) async-start(), calls=%async_computation.3 | async-start | bytes 6488064 | tf_op jit(solution)/shard_map/all_gather | solution.py:211
  215.5 199.7 %reduce-scatter.2.cloned.1.call-start = ((), (), s32[]{:S(2)}) async-start(), calls=%async_computation.4 | async-start | bytes 3932160 | tf_op jit(solution)/shard_map/reduce_scatter | solution.py:284
  274.4 1.7 copy-start.6
Sparse Core Ops, SparseCore 0:
  13.7 82.0 all-gather.5
  214.3 23.1 all-gather.11
  239.1 28.4 all-gather.7
  269.6 92.3 all-gather.9
  379.1 36.0 reduce-scatter.1

commit v2 on v1

--- a/solution.py
+++ b/solution.py
@@ -57,14 +57,16 @@
     return jnp.where(place < count // 2, 2 * place, 2 * (count - 1 - place) + 1)
 
 
-def attend_and_gather(count, shapes, *refs):
-    (shared, expand_key, expand_value, query_small, query_large, gate, up) = refs[:7]
-    out, gate_all, up_all = refs[7:10]
-    maxima, sums, send_sem, recv_sem, own_sem = refs[10:]
+def attend_and_gather(count, owners, shapes, *refs):
+    (shared, expand_key, expand_value, query_small, query_large, resid, gate, up, down) = refs[:9]
+    attn_all, resid_all, gate_all, up_all, down_all = refs[9:14]
+    out, maxima, sums, send_sem, recv_sem, own_sem, peer_send, peer_recv = refs[14:]
+    column = lax.axis_index("tp")
     me = lax.axis_index("sp")
     place = ring_place(me, count)
     right, left = ring_index(place + 1, count), ring_index(place - 1, count)
-    weights, wholes = (gate, up), (gate_all, up_all)
+    weights, wholes = (gate, up, down), (gate_all, up_all, down_all)
+    parts = len(weights)
     depth = gate.shape[0]
     half = depth // 2
     last = count // 2
@@ -74,7 +76,24 @@
         pl.semaphore_signal(
             barrier, inc=1, device_id={"sp": side}, device_id_type=pl.DeviceIdType.MESH
         )
-    pl.semaphore_wait(barrier, 2)
+    for ahead in range(1, owners):
+        pl.semaphore_signal(
+            barrier,
+            inc=1,
+            device_id={"tp": lax.rem(column + ahead, owners)},
+            device_id_type=pl.DeviceIdType.MESH,
+        )
+    pl.semaphore_wait(barrier, 1 + owners)
+
+    def share(source, whole, ahead, which):
+        return pltpu.make_async_remote_copy(
+            src_ref=source,
+            dst_ref=whole.at[column],
+            send_sem=peer_send.at[which, ahead],
+            recv_sem=peer_recv.at[which, ahead],
+            device_id={"tp": lax.rem(column + ahead, owners)},
+            device_id_type=pl.DeviceIdType.MESH,
+        )
 
     def hop(way, step, which):
         origin = ring_index(place - (step - 1) if way == 0 else place + (step - 1), count)
@@ -95,13 +114,19 @@
     def own(which):
         return pltpu.make_async_copy(weights[which], wholes[which].at[me], own_sem.at[which])
 
-    for which in range(2):
+    keep_resid = pltpu.make_async_copy(resid, resid_all.at[column], own_sem.at[parts])
+    keep_attn = pltpu.make_async_copy(out, attn_all.at[column], own_sem.at[parts + 1])
+
+    for which in range(parts):
         for way in range(2):
             hop(way, 1, which).start()
-    for which in range(2):
+    for ahead in range(1, owners):
+        share(resid, resid_all, ahead, 0).start()
+    for which in range(parts):
         own(which).start()
-
-    events = [(step, which) for step in range(1, last) for which in range(2)]
+    keep_resid.start()
+
+    events = [(step, which) for step in range(1, last) for which in range(parts)]
 
     def forward(step, which):
         for way in range(2):
@@ -121,7 +146,7 @@
             ).astype(jnp.bfloat16)
             value = lax.dot_general(
                 expand_value[value_at : value_at + width, :],
-                latent,
+                latent[:, : expand_value.shape[1]],
                 (((1,), (1,)), ((), ())),
                 preferred_element_type=jnp.float32,
             ).astype(jnp.bfloat16)
@@ -166,13 +191,21 @@
 
     lax.fori_loop(0, me, step_of, 0)
     block(me, True)
+    for ahead in range(1, owners):
+        share(out, attn_all, ahead, 1).start()
+    keep_attn.start()
     for number, event in enumerate(events):
 
         @pl.when(me <= 2 * number + 2)
         def _():
             forward(*event)
 
-    for which in range(2):
+    keep_resid.wait()
+    keep_attn.wait()
+    for ahead in range(1, owners):
+        share(resid, resid_all, ahead, 0).wait()
+        share(out, attn_all, ahead, 1).wait()
+    for which in range(parts):
         own(which).wait()
         for way in range(2):
             hop(way, last, which).wait_recv()
@@ -182,6 +215,7 @@
 
 def on_device(
     count,
+    owners,
     resid,
     query_small,
     query_large,
@@ -205,10 +239,7 @@
     shared = jnp.concatenate(
         [norm_rows(kv_latent, kv_gain), rotate(rope_key, angle_cos, angle_sin)], axis=1
     )
-    shared = jnp.pad(lax.all_gather(shared, "sp", axis=0, tiled=True), ((0, 0), (0, 128 - ROTARY)))
-    resid, down_weight, shared = lax.optimization_barrier((resid, down_weight, shared))
-    resid_all = lax.all_gather(resid, "tp", axis=0, tiled=True)
-    down_whole = lax.all_gather(down_weight, "sp", axis=0, tiled=True)
+    shared = lax.all_gather(shared, "sp", axis=0, tiled=True)
 
     shapes = []
     queries, keys, values = [], [], []
@@ -227,33 +258,41 @@
         full = jnp.concatenate([shaped[..., :nope], turned], axis=-1)
         full = jnp.pad(full, ((0, 0), (0, 0), (0, padded - wide)))
         queries.append(jnp.transpose(full, (1, 2, 0)))
-        rotary_part = jnp.eye(128, padded, k=nope, dtype=jnp.bfloat16)
-        rotary_part = jnp.where(jnp.arange(128)[:, None] < ROTARY, rotary_part, 0)
+        rotary_part = jnp.eye(ROTARY, padded, k=nope, dtype=jnp.bfloat16)
         for head in range(heads):
             part = jnp.pad(up_key[:, head * nope : (head + 1) * nope], ((0, 0), (0, padded - nope)))
-            keys.append(jnp.concatenate([part, rotary_part.astype(jnp.bfloat16)], axis=0))
+            keys.append(jnp.concatenate([part, rotary_part], axis=0))
             shapes.append((group, head, nope, padded, key_at, width, value_at, sum_at, value_at))
             key_at += padded
             value_at += width
             sum_at += width + PAD
-        values.append(jnp.pad(jnp.transpose(up_value), ((0, 0), (0, 128))))
+        values.append(jnp.transpose(up_value))
     expand_key = jnp.concatenate(keys, axis=1)
     expand_value = jnp.concatenate(values, axis=0)
     depth, hidden_size = gate_weight.shape
     vmem = pl.BlockSpec(memory_space=pltpu.VMEM)
     hbm = pl.BlockSpec(memory_space=pl.ANY)
     whole = jax.ShapeDtypeStruct((count, depth, hidden_size), jnp.bfloat16)
-    attn, gate_whole, up_whole = pl.pallas_call(
-        functools.partial(attend_and_gather, count, tuple(shapes)),
-        out_shape=(jax.ShapeDtypeStruct((value_at, rows), jnp.bfloat16), whole, whole),
-        in_specs=[vmem] * 5 + [hbm] * 2,
-        out_specs=(vmem, hbm, hbm),
+    attn_all, resid_all, gate_whole, up_whole, down_whole = pl.pallas_call(
+        functools.partial(attend_and_gather, count, owners, tuple(shapes)),
+        out_shape=(
+            jax.ShapeDtypeStruct((owners, value_at, rows), jnp.bfloat16),
+            jax.ShapeDtypeStruct((owners,) + resid.shape, jnp.bfloat16),
+            whole,
+            whole,
+            whole,
+        ),
+        in_specs=[vmem] * 5 + [hbm] * 4,
+        out_specs=(hbm,) * 5,
         scratch_shapes=[
+            pltpu.VMEM((value_at, rows), jnp.bfloat16),
             pltpu.VMEM((len(shapes), 1, rows), jnp.float32),
             pltpu.VMEM((sum_at, rows), jnp.float32),
-            pltpu.SemaphoreType.DMA((2, count // 2, 2)),
-            pltpu.SemaphoreType.DMA((2, count // 2, 2)),
-            pltpu.SemaphoreType.DMA((2,)),
+            pltpu.SemaphoreType.DMA((2, count // 2, 3)),
+            pltpu.SemaphoreType.DMA((2, count // 2, 3)),
+            pltpu.SemaphoreType.DMA((5,)),
+            pltpu.SemaphoreType.DMA((2, owners)),
+            pltpu.SemaphoreType.DMA((2, owners)),
         ],
         compiler_params=pltpu.CompilerParams(
             collective_id=0, has_side_effects=True, vmem_limit_bytes=50 * 2**20
@@ -261,11 +300,22 @@
         cost_estimate=pl.CostEstimate(
             flops=10**11, bytes_accessed=3 * 10**7, transcendentals=2 * 10**7
         ),
-    )(shared, expand_key, expand_value, queries[0], queries[1], gate_weight, up_weight)
+    )(
+        shared,
+        expand_key,
+        expand_value,
+        queries[0],
+        queries[1],
+        resid,
+        gate_weight,
+        up_weight,
+        down_weight,
+    )
+    resid_all = resid_all.reshape(rows, resid.shape[1])
+    down_whole = down_whole.reshape(count * depth, hidden_size)
     gate_whole = gate_whole.reshape(count * depth, hidden_size)
     up_whole = up_whole.reshape(count * depth, hidden_size)
     border_device = up_value_small.shape[1]
-    attn_all = lax.all_gather(attn, "tp", axis=0)
     attn_small = attn_all[:, :border_device].reshape(-1, rows)
     attn_large = attn_all[:, border_device:].reshape(-1, rows)
     border = HEADS_SMALL * VALUE_SMALL
@@ -314,5 +364,5 @@
         P("sp", "tp"),
     )
     return jax.shard_map(
-        functools.partial(on_device, mesh.shape["sp"]), mesh=mesh, in_specs=placed, out_specs=P(("sp", "tp"), None), check_vma=False
-    )
+        functools.partial(on_device, mesh.shape["sp"], mesh.shape["tp"]), mesh=mesh, in_specs=placed, out_specs=P(("sp", "tp"), None), check_vma=False
+    )

time: 425 us -> 345 us (0.81)
  waiting for transfers between devices: 236 us -> 112 us
  Pallas kernels: 113 us -> 169 us
  matrix products: 41.1 us -> 30.6 us
    all_gather x4 -> x1, waiting for transfers between devices: 199 us -> 75.6 us  [on_device(): shared = lax.all_gather(shared, 'sp', axis=0, tiled=True)]
    pallas_call x1, Pallas kernels: 113 us -> 169 us  [on_device(): pl.pallas_call(functools.partial(attend_and_gather, count, owners, tuple(...]
    pad x1 -> x0, local copies, waits for them, and re-layouts: 4.99 us -> none  [on_device(): jnp.pad(lax.all_gather(shared, 'sp', axis=0, tiled=True), ((0, 0), (0, 12...]
  transfers between devices with their start and end apart: 5 -> 2, of which waited for: 5 -> 2; matrix products, arithmetic and copies ran while one was open for 7% -> 2% of each run, Pallas kernels for 0% -> 0%
where the time goes in v2:
time: 345 us; the launch traced here: 344 us
  Pallas kernels  169 us (49%)
  waiting for transfers between devices  112 us (32%)
  matrix products  30.6 us (9%)
  between operations  13.7 us (4%)
  other arithmetic  10.9 us (3%)
  local copies, waits for them, and re-layouts  8.51 us (2%)
    pallas_call x1, Pallas kernels, on_device(): pl.pallas_call(functools.partial(attend_and_gather, count, owners, tuple(...  169 us
    all_gather x1, waiting for transfers between devices, on_device(): shared = lax.all_gather(shared, 'sp', axis=0, tiled=True)  75.6 us
    reduce_scatter x1, waiting for transfers between devices, on_device(): lax.psum_scatter(lax.dot_general(hidden, down_whole, (((1,), (1,)), ((),...  36 us
    dot_general x1, matrix products, on_device(): lax.dot_general(hidden, down_whole, (((1,), (1,)), ((), ())), preferred_e...  17.3 us
    dot_general x1, matrix products, on_device(): gate = jnp.dot(mixer_in, gate_whole, preferred_element_type=jnp.float32)  7.04 us
  transfers between devices with their start and end apart: 2, of which 2 were waited for; matrix products, arithmetic and copies ran while one was open for 2% of the time, Pallas kernels for 0%

profile of v2, /device:TPU:0, one launch (start us, length us, event | category | flops | bytes accessed | tf_op | source)
XLA Modules:
  0.0 344.2 jit_solution(14600050633199155694)
XLA Ops:
  6.5 0.0 all-gather.2.cloned.1.call-start
  6.5 0.8 slice_convert_fusion
  7.3 0.2 copy.22
  7.5 0.2 copy.23
  7.7 1.2 fusion.22
  8.9 0.7 convert_element_type.98
  9.5 1.2 fusion.24
  10.7 0.0 copy-start.8
  10.7 0.0 copy-start.4
  10.7 0.0 copy-start.7
  10.7 1.8 multiply_cosine_fusion
  12.5 0.0 copy-start.5
  12.5 0.0 slice-start
  12.5 0.0 copy-start
  12.5 0.0 copy-start.1
  12.5 0.9 pad_maximum_fusion
  13.5 0.0 all-gather.2.cloned.1.call-update
  13.5 0.0 reduce-scatter.2.cloned.1.call-start
  13.6 0.1 copy.27
  13.7 0.1 copy.28
  13.8 1.0 slice.69
  14.9 0.9 slice.66
  15.8 0.9 slice.54
  16.7 1.0 copy.26
  17.8 0.0 copy-done.5
  17.8 0.1 copy.25
  17.9 0.0 copy-done.6
  17.9 0.9 fusion.48
  18.9 0.1 fusion.27.refs_4_
  19.0 0.1 fusion.52
  19.1 0.1 fusion.51
  19.1 0.9 broadcast_select_fusion.1
  20.0 0.0 copy-done.4
  20.1 75.6 %all-gather.2.cloned.1.call-done.refs_0_ = bf16[6144,288]{1,0:T(8,128)(2,1)} async-done(((bf16[768,288]{1,0:T(8,128)(2,1)}), bf16[6144,288]{1,0:T(8,128)(2,1)}) %all-gather.2.cloned.1.call-update) | async-done | bytes 3538960 | tf_op jit(solution)/shard_map/all_gather | solution.py:242
  95.7 0.0 copy-done
  95.7 1.1 copy-done.2
  96.8 168.8 %shard_map.145 = (bf16[4,384,768]{2,1,0:T(8,128)(2,1)}, bf16[4,192,2048]{2,1,0:T(8,128)(2,1)}, bf16[8,256,1408]{2,1,0:T(8,128)(2,1)}, bf16[8,256,1408]{2,1,0:T(8,128)(2,1)}, bf16[8,256,1408]{2,1,0:T(8,128)(2,1)}) custom-call(bf16[6144,288]{1,0:T(8,128)(2,1)} %all-gather.2.cloned.1.call-done.refs_0_, bf16[288,768]{1,0:T(8,128)(2,1)S(1)} %fusion.32.refs_1_, ...), custom_call_target="tpu_custom_call" | custom-call | flops 99999997952 | bytes 30000000 | tf_op jit(solution)/shard_map/pallas_call | solution.py:276
  265.6 1.5 slice.64
  267.1 1.2 slice.62
  268.4 0.0 slice-start.1
  268.4 3.6 %fusion.4 = f32[768,2048]{1,0:T(8,128)S(1)} fusion(bf16[1024,768]{1,0:T(8,128)(2,1)S(1)} %bitcast.20, bf16[1536,2048]{1,0:T(8,128)(2,1)S(1)} %copy-done.3), kind=kOutput, calls=%fused_computation.8 | convolution fusion | flops 3221225472 | bytes 12058624 | tf_op jit(solution)/shard_map/dot_general | solution.py:326
  271.9 0.0 slice-start.2
  271.9 2.7 fusion
  274.7 7.0 %fusion.11 = f32[768,1408]{1,0:T(8,128)} fusion(bf16[2048,1408]{1,0:T(8,128)(2,1)S(1)} %bitcast.32, bf16[768,2048]{1,0:T(8,128)(2,1)S(1)} %get-tuple-element.30, f32[2048]{0:T(1024)S(1)} %convert_element_type.115, f32[768]{0:T(1024)S(1)} %add_rsqrt_fusion), kind=kOutput, calls=%fused_computation.21 | convolution fusion | flops 4435476480 | bytes 13249536 | tf_op jit(solution)/shard_map/dot_general | solution.py:331
  281.7 17.3 %convolution_convert_fusion = bf16[768,2048]{1,0:T(8,128)(2,1)} fusion(bf16[2048,1408]{1,0:T(8,128)(2,1)} %bitcast.29, f32[768,1408]{1,0:T(8,128)} %fusion.11, bf16[2048,1408]{1,0:T(8,128)(2,1)} %bitcast.28, bf16[768,2048]{1,0:T(8,128)(2,1)S(1)} %get-tuple-element.30, f32[2048]{0:T(1024)S(1)} %convert_element_type.115, f32[768]{0:T(1024)S(1)} %add_rsqrt_fusion), kind=kOutput, calls=%fused_computation.10 | convolution fusion | flops 8872722432 | bytes 22162432 | tf_op jit(solution)/shard_map/dot_general | solution.py:335
  299.0 0.0 reduce-scatter.2.cloned.1.call-update
  299.1 36.0 %reduce-scatter.2.cloned.1.call-done = bf16[192,2048]{1,0:T(8,128)(2,1)} async-done(((bf16[768,2048]{1,0:T(8,128)(2,1)}), bf16[192,2048]{1,0:T(8,128)(2,1)}) %reduce-scatter.2.cloned.1.call-update) | async-done | bytes 786448 | tf_op jit(solution)/shard_map/reduce_scatter | solution.py:334
  335.1 2.3 add_convert_fusion
  (24 shorter events, 0.2 us)
Async XLA Ops:
  6.5 11.3 %copy-start.6 = (bf16[2048]{0:T(1024)(128)(2,1)S(1)}, bf16[2048]{0:T(1024)(128)(2,1)}, u32[]{:S(2)}) copy-start(bf16[2048]{0:T(1024)(128)(2,1)} %param.26) | copy-start | bytes 12292
  6.5 89.2 %all-gather.2.cloned.1.call-start = ((), (), s32[]{:S(2)}) async-start(), calls=%async_computation.1 | async-start | bytes 5308416 | tf_op jit(solution)/shard_map/all_gather | solution.py:242
  10.7 8.4 %copy-start.8 = (pred[128]{0:T(512)(128)(4,1)S(1)}, pred[128]{0:T(512)(128)(4,1)}, u32[]{:S(2)}) copy-start(pred[128]{0:T(512)(128)(4,1)} %constant.35.clone.1) | copy-start | bytes 388
  10.7 9.3 %copy-start.4 = (bf16[256,256]{1,0:T(8,128)(2,1)S(1)}, bf16[256,256]{1,0:T(8,128)(2,1)}, u32[]{:S(2)}) copy-start(bf16[256,256]{1,0:T(8,128)(2,1)} %param.23) | copy-start | bytes 393220
  10.7 9.3 %copy-start.7 = (pred[256]{0:T(512)(128)(4,1)S(1)}, pred[256]{0:T(512)(128)(4,1)}, u32[]{:S(2)}) copy-start(pred[256]{0:T(512)(128)(4,1)} %constant.38.clone.1) | copy-start | bytes 772
  12.5 5.3 %copy-start.5 = (bf16[256,128]{1,0:T(8,128)(2,1)S(1)}, bf16[256,128]{1,0:T(8,128)(2,1)}, u32[]{:S(2)}) copy-start(bf16[256,128]{1,0:T(8,128)(2,1)} %param.22) | copy-start | bytes 196612
  12.5 7.5 %slice-start = ((bf16[256,256]{1,0:T(8,128)(2,1)}), bf16[256,128]{1,0:T(8,128)(2,1)S(1)}, s32[]{:S(2)}) async-start(bf16[256,256]{1,0:T(8,128)(2,1)} %param.23), calls=%async_computation.3 | async-start | bytes 131072 | tf_op jit(solution)/shard_map/slice | solution.py:263
  12.5 83.2 %copy-start = (bf16[256,1408]{1,0:T(8,128)(2,1)S(1)}, bf16[256,1408]{1,0:T(8,128)(2,1)}, u32[]{:S(2)}) copy-start(bf16[256,1408]{1,0:T(8,128)(2,1)} %refs_6_.1) | copy-start | bytes 2162692
  12.5 83.2 %copy-start.1 = (bf16[256,1408]{1,0:T(8,128)(2,1)S(1)}, bf16[256,1408]{1,0:T(8,128)(2,1)}, u32[]{:S(2)}) copy-start(bf16[256,1408]{1,0:T(8,128)(2,1)} %refs_7_.1) | copy-start | bytes 2162692
  13.5 321.6 %reduce-scatter.2.cloned.1.call-start = ((), (), s32[]{:S(2)}) async-start(), calls=%async_computation.2 | async-start | bytes 3932160 | tf_op jit(solution)/shard_map/reduce_scatter | solution.py:334
  95.7 1.1 copy-start.2
  96.8 171.5 %copy-start.3 = (bf16[1536,2048]{1,0:T(8,128)(2,1)S(1)}, bf16[1536,2048]{1,0:T(8,128)(2,1)}, u32[]{:S(2)}) copy-start(bf16[1536,2048]{1,0:T(8,128)(2,1)} %param.25) | copy-start | bytes 18874372
  268.3 3.6 %copy-start.9 = (bf16[4,192,2048]{2,1,0:T(8,128)(2,1)S(1)}, bf16[4,192,2048]{2,1,0:T(8,128)(2,1)}, u32[]{:S(2)}) copy-start(bf16[4,192,2048]{2,1,0:T(8,128)(2,1)} %get-tuple-element.10) | copy-start | bytes 9437188
  268.4 6.3 %slice-start.1 = ((s8[5767168]{0:T(1024)(128)(4,1)}), s8[4194304]{0:T(1024)(128)(4,1)S(1)}, s32[]{:S(2)}) async-start(s8[5767168]{0:T(1024)(128)(4,1)} %bitcast.30), calls=%async_computation.4 | async-start | bytes 8388608
  271.9 2.7 slice-start.2
Sparse Core Ops, SparseCore 0:
  13.6 82.0 all-gather.1
  299.2 35.8 reduce-scatter.1
